TPU v7x, 512 devices: a whole 4x8x8 slice. The times are simulated.
512 devices in a mesh: fs: 64 (over z, y), tp: 8 (over x, core).
Axes of the slice: x: 4, y: 8, z: 8, core: 2. Of those that a mesh axis runs over, the one named last changes fastest.
Arguments:
- inputs: bfloat16 [32768, 2048], P('fs', 'tp'), may hold values from -6 to 6
- value_cotangent: bfloat16 [32768, 2048], P('fs', 'tp'), may hold values from -6 to 6
- first_map: bfloat16 [32768, 2048], P('fs', 'tp'), may hold values from -6 to 6
- second_map: bfloat16 [32768, 2048], P('fs', 'tp'), may hold values from -6 to 6
- lambdas: float32 [16], P('tp'), may hold values from 0.3 to 0.8
- head_gain: float32 [128], replicated, may hold values from 0.1 to 1.9
- output_cotangent: bfloat16 [32768, 2048], P('fs', 'tp'), may hold values from -6 to 6
- value_factor: bfloat16 [2048, 256], replicated, may hold values from -0.125 to 0.125
- output_factor: bfloat16 [2048, 256], replicated, may hold values from -0.125 to 0.125
- value_weight: float32 [2048, 2048], P('fs', 'tp'), may hold values from -0.125 to 0.125
- output_weight: float32 [2048, 2048], P('tp', 'fs'), may hold values from -0.125 to 0.125
- value_moment: float32 [256, 2048], P('fs', 'tp'), may hold values from -6 to 6
- value_second: float32 [256, 2048], P('fs', 'tp'), may hold values from 0.25 to 4
- output_moment: float32 [256, 2048], P('fs', 'tp'), may hold values from -6 to 6
- output_second: float32 [256, 2048], P('fs', 'tp'), may hold values from 0.25 to 4
Outputs:
- value_master: float32 [2048, 2048], P('fs', 'tp')
- output_master: float32 [2048, 2048], P('tp', 'fs')
- value_moment_new: float32 [256, 2048], P('fs', 'tp')
- value_second_new: float32 [256, 2048], P('fs', 'tp')
- output_moment_new: float32 [256, 2048], P('fs', 'tp')
- output_second_new: float32 [256, 2048], P('fs', 'tp')
- value_copy: bfloat16 [2048, 2048], P(None, 'tp')
- output_copy: bfloat16 [2048, 2048], P('tp')
All inputs are finite; a program needn't handle non-finite values.
Results may differ from a plain program's by a relative error of at most 0.0027.
Values may be sent and summed in bfloat16 or wider, within the bound.
No kernel may reach another device: no remote copies, remote signals or barrier semaphores. Data moves between devices by JAX's collectives and lax.ppermute only.
A program may use at most 64 MiB of HBM per device.

v0:
```python
import math
import jax
import jax.numpy as jnp
from jax import lax
from jax.sharding import PartitionSpec as P


def side_by_side(arrays, axis, dim, along):
    ends, at = ([], 0)
    for a in arrays[:-1]:
        at += a.shape[along]
        ends.append(at)
    both = jnp.concatenate(arrays, axis=along)
    return tuple(jnp.split(lax.all_gather(both, axis, axis=dim, tiled=True), ends, axis=along))


def cut_along(x, dim, size):
    before, after = (x.shape[:dim], x.shape[dim + 1 :])
    return jnp.moveaxis(x.reshape(*before, size, -1, *after), dim, 0)


def sum_at_owner(x, axis, dim):
    size = lax.axis_size(axis)
    tiles = lax.all_to_all(cut_along(x, dim, size), axis, 0, 0, tiled=True)
    return jnp.sum(tiles.astype(jnp.float32), axis=0)


def laid_out(tiles, dim):
    tiles = jnp.moveaxis(tiles, 0, dim)
    lengths = tiles.shape
    return tiles.reshape(*lengths[:dim], lengths[dim] * lengths[dim + 1], *lengths[dim + 2 :])


def copy_for_each(x, axis):
    size = lax.axis_size(axis)
    return lax.all_to_all(jnp.broadcast_to(x[None], (size, *x.shape)), axis, 0, 0, tiled=True)


def gathered_copies(x, axis, dim):
    return laid_out(copy_for_each(x, axis), dim)


def gather_turned(arrays, axis, dims):
    turned = [jnp.moveaxis(a, dim, 0) for a, dim in zip(arrays, dims)]
    both = jnp.concatenate([t.reshape(len(t), -1) for t in turned], axis=1)
    filled, at, done = (lax.all_gather(both, axis, axis=0, tiled=True), 0, [])
    for t, dim in zip(turned, dims):
        slab = filled[:, at : at + t[0].size].reshape(-1, *t.shape[1:])
        done.append(jnp.moveaxis(slab, 0, dim))
        at += t[0].size
    return tuple(done)


def contract_rows(left, right, precise):
    if precise:
        return lax.dot_general(
            left,
            right,
            (((0,), (0,)), ((), ())),
            precision=lax.Precision.HIGHEST,
            preferred_element_type=jnp.float32,
        )
    return lax.dot_general(
        left, right, (((0,), (0,)), ((), ())), preferred_element_type=jnp.float32
    )


def local(
    inputs,
    value_cotangent,
    first_map,
    second_map,
    lambdas,
    head_gain,
    output_cotangent,
    value_factor,
    output_factor,
    value_weight,
    output_weight,
    value_moment,
    value_second,
    output_moment,
    output_second,
):
    tok_rows = inputs.shape[0]
    local_heads = lambdas.shape[0]
    head_width = head_gain.shape[0]
    head_cols = local_heads * head_width
    first = first_map.astype(jnp.float32).reshape(tok_rows, local_heads, head_width)
    second = second_map.astype(jnp.float32).reshape(tok_rows, local_heads, head_width)
    difference = first - lambdas[None, :, None] * second
    normed = (
        difference
        * lax.rsqrt(jnp.mean(difference * difference, axis=-1, keepdims=True) + 1e-06)
        * head_gain
    )
    heads_out = normed.reshape(tok_rows, head_cols).astype(jnp.bfloat16)
    full_inputs, full_cotangent = side_by_side((inputs, output_cotangent), "tp", 1, 0)
    token_scale = 1.0 / math.sqrt(tok_rows * lax.axis_size("fs"))
    fs_index = lax.axis_index("fs")
    width_rows = value_weight.shape[0]
    value_rows = lax.dynamic_slice_in_dim(
        value_factor, fs_index * width_rows, width_rows, 0
    ).astype(jnp.float32)
    output_rows = lax.dynamic_slice_in_dim(
        output_factor, fs_index * width_rows, width_rows, 0
    ).astype(jnp.float32)
    grad_value = contract_rows(full_inputs, value_cotangent, False) * token_scale
    grad_output = contract_rows(full_cotangent, heads_out, False) * token_scale
    partial_value = jnp.concatenate(
        [
            contract_rows(value_factor.astype(jnp.float32), grad_value, True),
            contract_rows(output_factor.astype(jnp.float32), grad_output, True),
        ],
        axis=1,
    )
    own_rows = sum_at_owner(partial_value.astype(jnp.bfloat16), "fs", 0)
    moments = jnp.concatenate([value_moment, output_moment], axis=1)
    seconds = jnp.concatenate([value_second, output_second], axis=1)
    moment_new = 0.8 * moments + 0.2 * own_rows
    second_new = 0.95 * seconds + 0.05 * own_rows * own_rows
    direction = moment_new / (jnp.sqrt(second_new) + 1e-08)
    full_direction = gathered_copies(direction, "fs", 0)
    step_value = jnp.dot(
        value_rows,
        full_direction[:, :head_cols],
        precision=lax.Precision.HIGHEST,
        preferred_element_type=jnp.float32,
    )
    step_output = jnp.dot(
        output_rows,
        full_direction[:, head_cols:],
        precision=lax.Precision.HIGHEST,
        preferred_element_type=jnp.float32,
    )
    value_master = value_weight - 0.05 * step_value
    output_master = output_weight - 0.05 * step_output.T
    value_copy, output_copy = gather_turned(
        (value_master.astype(jnp.bfloat16), output_master.astype(jnp.bfloat16)), "fs", (0, 1)
    )
    return (
        value_master,
        output_master,
        moment_new[:, :head_cols],
        second_new[:, :head_cols],
        moment_new[:, head_cols:],
        second_new[:, head_cols:],
        value_copy,
        output_copy,
    )


def solution(mesh):
    in_specs = (
        P("fs", "tp"),
        P("fs", "tp"),
        P("fs", "tp"),
        P("fs", "tp"),
        P("tp"),
        P(),
        P("fs", "tp"),
        P(),
        P(),
        P("fs", "tp"),
        P("tp", "fs"),
        P("fs", "tp"),
        P("fs", "tp"),
        P("fs", "tp"),
        P("fs", "tp"),
    )
    out_specs = (
        P("fs", "tp"),
        P("tp", "fs"),
        P("fs", "tp"),
        P("fs", "tp"),
        P("fs", "tp"),
        P("fs", "tp"),
        P(None, "tp"),
        P("tp", None),
    )
    return jax.shard_map(local, mesh=mesh, in_specs=in_specs, out_specs=out_specs, check_vma=False)
```

profile of v0, /device:TPU:2, one launch (start us, length us, event | category | flops | bytes accessed | tf_op | source)
XLA Modules:
  0.0 207.0 jit_solution(13290908280082833347)
XLA Ops:
  7.2 0.0 copy-start
  7.2 0.0 copy-start.3
  7.2 0.0 copy-start.11
  7.2 0.0 copy-start.12
  7.2 0.0 all-gather.3.cloned.1.call-start
  7.3 1.9 pad_maximum_fusion
  9.2 0.0 all-gather.3.cloned.1.call-update
  9.2 0.0 copy-start.2
  9.2 1.3 reshape.84
  10.5 0.0 copy-done.3
  10.5 0.3 reshape.85
  10.8 0.0 copy-done.11
  10.8 0.7 multiply_reduce_fusion
  11.5 0.0 copy-done.12
  11.5 0.1 broadcast_bitcast_fusion
  11.6 44.3 %all-gather.3.cloned.1.call-done = bf16[1024,2048]{1,0:T(8,128)(2,1)} async-done(((bf16[1024,256]{1,0:T(8,128)(2,1)}), bf16[1024,2048]{1,0:T(8,128)(2,1)}) %all-gather.3.cloned.1.call-update) | async-done | bytes 4194320 | tf_op jit(solution)/shard_map/all_gather | solution.py:14
  55.9 0.6 mul.124
  56.5 0.0 copy-done.2
  56.6 0.0 copy-start.1
  56.6 2.5 %convolution_multiply_fusion = f32[2048,256]{1,0:T(8,128)S(1)} fusion(bf16[1024,2048]{1,0:T(8,128)(2,1)} %all-gather.3.cloned.1.call-done, f32[64,8,2,128]{3,2,1,0:T(2,128)S(1)} %bitcast.25, f32[256]{0:T(256)S(1)} %get-tuple-element.43, f32[256]{0:T(256)S(1)} %get-tuple-element.44, bf16[512,256]{1,0:T(8,128)(2,1)S(1)} %copy-done.3, ...), kind=kOutput, calls=%fused_computation | convolution fusion | flops 538312704 | bytes 5244928 | tf_op jit(solution)/shard_map/dot_general | solution.py:63
  59.1 0.0 copy-done.1
  59.1 0.0 copy-start.13
  59.1 1.5 fusion.3
  60.7 0.0 copy-done.13
  60.7 2.3 %convolution_multiply_fusion.1 = f32[2048,256]{1,0:T(8,128)S(1)} fusion(bf16[512,256]{1,0:T(8,128)(2,1)S(1)} %copy-done.13, bf16[1024,2048]{1,0:T(8,128)(2,1)} %all-gather.3.cloned.1.call-done), kind=kOutput, calls=%fused_computation.1 | convolution fusion | flops 537395200 | bytes 4456448 | tf_op jit(solution)/shard_map/dot_general | solution.py:63
  63.0 0.0 copy-done
  63.0 0.0 copy-start.7
  63.0 0.0 copy-start.8
  63.1 0.0 copy-start.9
  63.1 0.0 copy-start.10
  63.1 1.5 fusion.2
  64.6 0.0 copy-start.5
  64.6 0.0 copy-start.6
  64.6 0.1 pad_maximum_fusion.1
  64.8 28.4 %all_to_all.10 = bf16[64,4,512]{2,1,0:T(4,128)(2,1)S(1)} all-to-all(bf16[64,4,512]{2,1,0:T(4,128)(2,1)S(1)} %pad_maximum_fusion.1), channel_id=1, replica_groups=mesh['fs'=64,'tp'=8] {'fs'}, dimensions={0} | all-to-all | bytes 524288 | tf_op jit(solution)/shard_map/all_to_all | solution.py:24
  93.2 0.1 convert_reduce_fusion
  93.3 0.0 copy-done.7
  93.3 0.0 copy-done.8
  93.3 0.0 copy-done.9
  93.3 0.0 copy-done.10
  93.4 0.9 broadcast_in_dim.2
  94.3 4.6 %all-to-all-start.1 = ((f32[64,4,512]{2,1,0:T(4,128)}), f32[64,4,512]{2,1,0:T(4,128)S(1)}, u32[]{:S(2)}, u32[]{:S(2)}) async-start(f32[64,4,512]{2,1,0:T(4,128)} %broadcast_in_dim.2), calls=%async_computation.1 | async-start | bytes 1048576 | tf_op jit(solution)/shard_map/all_to_all | solution.py:36
  98.9 0.0 all-gather.5.cloned.1.call-start
  98.9 18.6 %all-to-all-done.1 = f32[64,4,512]{2,1,0:T(4,128)S(1)} async-done(((f32[64,4,512]{2,1,0:T(4,128)}), f32[64,4,512]{2,1,0:T(4,128)S(1)}, u32[]{:S(2)}, u32[]{:S(2)}) %all-to-all-start.1) | async-done | bytes 524320 | tf_op jit(solution)/shard_map/all_to_all | solution.py:36
  117.5 0.2 reshape.86
  117.7 0.0 copy-done.5
  117.7 0.2 fusion.4
  118.0 0.0 copy-start.4
  118.0 0.0 copy-done.6
  118.0 0.9 fusion.25
  118.9 0.6 pad_maximum_fusion.2
  119.5 0.0 all-gather.5.cloned.1.call-update
  119.5 0.6 fusion.23
  120.1 0.6 fusion.24
  120.7 75.4 %all-gather.5.cloned.1.call-done = bf16[2048,512]{1,0:T(8,128)(2,1)} async-done(((bf16[32,512]{1,0:T(8,128)(2,1)}), bf16[2048,512]{1,0:T(8,128)(2,1)}) %all-gather.5.cloned.1.call-update) | async-done | bytes 2097168 | tf_op jit(solution)/shard_map/all_gather | solution.py:46
  196.1 2.6 %slice_bitcast_fusion = (bf16[256,2048]{0,1:T(8,128)(2,1)S(1)}, bf16[2048,256]{1,0:T(8,128)(2,1)}) fusion(bf16[2048,512]{1,0:T(8,128)(2,1)} %all-gather.5.cloned.1.call-done), kind=kLoop, calls=%fused_computation.12 | loop fusion | bytes 4194304 | tf_op jit(solution)/shard_map/transpose | solution.py:49
  198.8 0.0 copy-done.4
  198.8 1.4 copy.28
  (5 shorter events, 0.1 us)
Async XLA Ops:
  7.2 55.9 %copy-start = (bf16[2048,256]{1,0:T(8,128)(2,1)S(1)}, bf16[2048,256]{1,0:T(8,128)(2,1)}, u32[]{:S(2)}) copy-start(bf16[2048,256]{1,0:T(8,128)(2,1)} %param.22) | copy-start | bytes 3145732
  7.2 3.3 %copy-start.3 = (bf16[512,256]{1,0:T(8,128)(2,1)S(1)}, bf16[512,256]{1,0:T(8,128)(2,1)}, u32[]{:S(2)}) copy-start(bf16[512,256]{1,0:T(8,128)(2,1)} %param.18) | copy-start | bytes 786436
  7.2 3.6 %copy-start.11 = (f32[2]{0:T(128)S(1)}, f32[2]{0:T(128)}, u32[]{:S(2)}) copy-start(f32[2]{0:T(128)} %param.19) | copy-start | bytes 28
  7.2 4.3 %copy-start.12 = (f32[128]{0:T(128)S(1)}, f32[128]{0:T(128)}, u32[]{:S(2)}) copy-start(f32[128]{0:T(128)} %param.20) | copy-start | bytes 1540
  7.2 48.7 %all-gather.3.cloned.1.call-start = ((), (), s32[]{:S(2)}) async-start(), calls=%async_computation.2 | async-start | bytes 4718592 | tf_op jit(solution)/shard_map/all_gather | solution.py:14
  9.2 47.3 %copy-start.2 = (bf16[512,256]{1,0:T(8,128)(2,1)S(1)}, bf16[512,256]{1,0:T(8,128)(2,1)}, u32[]{:S(2)}) copy-start(bf16[512,256]{1,0:T(8,128)(2,1)} %param.17) | copy-start | bytes 786436
  56.6 2.5 %copy-start.1 = (bf16[2048,256]{1,0:T(8,128)(2,1)S(1)}, bf16[2048,256]{1,0:T(8,128)(2,1)}, u32[]{:S(2)}) copy-start(bf16[2048,256]{1,0:T(8,128)(2,1)} %param.23) | copy-start | bytes 3145732
  59.1 1.6 copy-start.13
  63.0 30.3 %copy-start.7 = (f32[4,256]{1,0:T(4,128)S(1)}, f32[4,256]{1,0:T(4,128)}, u32[]{:S(2)}) copy-start(f32[4,256]{1,0:T(4,128)} %param.29) | copy-start | bytes 12292
  63.0 30.3 %copy-start.8 = (f32[4,256]{1,0:T(4,128)S(1)}, f32[4,256]{1,0:T(4,128)}, u32[]{:S(2)}) copy-start(f32[4,256]{1,0:T(4,128)} %param.27) | copy-start | bytes 12292
  63.1 30.3 %copy-start.9 = (f32[4,256]{1,0:T(4,128)S(1)}, f32[4,256]{1,0:T(4,128)}, u32[]{:S(2)}) copy-start(f32[4,256]{1,0:T(4,128)} %param.28) | copy-start | bytes 12292
  63.1 30.3 %copy-start.10 = (f32[4,256]{1,0:T(4,128)S(1)}, f32[4,256]{1,0:T(4,128)}, u32[]{:S(2)}) copy-start(f32[4,256]{1,0:T(4,128)} %param.26) | copy-start | bytes 12292
  64.6 53.2 %copy-start.5 = (f32[256,32]{0,1:T(8,128)S(1)}, f32[256,32]{0,1:T(8,128)}, u32[]{:S(2)}) copy-start(f32[256,32]{0,1:T(8,128)} %param.25) | copy-start | bytes 98308
  64.6 53.4 %copy-start.6 = (f32[32,256]{1,0:T(8,128)S(1)}, f32[32,256]{1,0:T(8,128)}, u32[]{:S(2)}) copy-start(f32[32,256]{1,0:T(8,128)} %param.24) | copy-start | bytes 98308
  94.3 23.3 %all-to-all-start.1 = ((f32[64,4,512]{2,1,0:T(4,128)}), f32[64,4,512]{2,1,0:T(4,128)S(1)}, u32[]{:S(2)}, u32[]{:S(2)}) async-start(f32[64,4,512]{2,1,0:T(4,128)} %broadcast_in_dim.2), calls=%async_computation.1 | async-start | bytes 1048576 | tf_op jit(solution)/shard_map/all_to_all | solution.py:36
  98.9 97.2 %all-gather.5.cloned.1.call-start = ((), (), s32[]{:S(2)}) async-start(), calls=%async_computation.3 | async-start | bytes 2129920 | tf_op jit(solution)/shard_map/all_gather | solution.py:46
  118.0 80.8 %copy-start.4 = (f32[256,32]{0,1:T(8,128)}, f32[256,32]{0,1:T(8,128)S(1)}, u32[]{:S(2)}) copy-start(f32[256,32]{0,1:T(8,128)S(1)} %fusion.4) | copy-start | bytes 98308
Sparse Core Ops, SparseCore 0:
  10.7 45.1 all-gather.2
  119.6 76.4 all-gather.4
where the time goes:
time: 207 us
  waiting for transfers between devices  138 us (67%)
  blocking collectives  28.4 us (14%)
  between operations  14.3 us (7%)
  matrix products  8.94 us (4%)
  local copies, waits for them, and re-layouts  8.65 us (4%)
  starting transfers between devices  4.71 us (2%)
  other arithmetic  3.6 us (2%)
    all_gather x1, waiting for transfers between devices, gather_turned(): filled, at, done = (lax.all_gather(both, axis, axis=0, tiled=True), 0, [])  75.4 us
    all_gather x1, waiting for transfers between devices, side_by_side(): lax.all_gather(both, axis, axis=dim, tiled=True)  44.3 us
    all_to_all x1, blocking collectives, sum_at_owner(): tiles = lax.all_to_all(cut_along(x, dim, size), axis, 0, 0, tiled=True)  28.4 us
    all_to_all x1, waiting for transfers between devices, copy_for_each(): lax.all_to_all(jnp.broadcast_to(x[None], (size, *x.shape)), axis, 0, 0, t...  18.6 us
    dot_general x2, matrix products, contract_rows(): lax.dot_general(left, right, (((0,), (0,)), ((), ())), preferred_element_...  4.85 us
    all_to_all x1, starting transfers between devices, copy_for_each(): lax.all_to_all(jnp.broadcast_to(x[None], (size, *x.shape)), axis, 0, 0, t...  4.63 us
  transfers between devices with their start and end apart: 3, of which 3 were waited for; matrix products, arithmetic and copies ran while one was open for 2% of the time, Pallas kernels for 0%

commit v1 on v0

--- a/solution.py
+++ b/solution.py
@@ -43,7 +43,16 @@
 def gather_turned(arrays, axis, dims):
     turned = [jnp.moveaxis(a, dim, 0) for a, dim in zip(arrays, dims)]
     both = jnp.concatenate([t.reshape(len(t), -1) for t in turned], axis=1)
-    filled, at, done = (lax.all_gather(both, axis, axis=0, tiled=True), 0, [])
+    filled, at, done = (
+        jnp.concatenate(
+            lax.all_to_all(
+                jnp.stack([both for _ in range(lax.axis_size(axis))], axis=0), axis, 0, 0
+            ),
+            axis=0,
+        ),
+        0,
+        [],
+    )
     for t, dim in zip(turned, dims):
         slab = filled[:, at : at + t[0].size].reshape(-1, *t.shape[1:])
         done.append(jnp.moveaxis(slab, 0, dim))

time: 207 us -> 188 us (0.908)
  waiting for transfers between devices: 138 us -> 113 us
  starting transfers between devices: 4.71 us -> 9.63 us
    all_gather x1 -> x0, waiting for transfers between devices: 75.4 us -> none  [gather_turned(): filled, at, done = (lax.all_gather(both, axis, axis=0, tiled=True), 0, [])]
    all_to_all x0 -> x1, waiting for transfers between devices: none -> 50.3 us  [gather_turned(): lax.all_to_all(jnp.stack([both for _ in range(lax.axis_size(axis))], axis...]
    all_to_all x0 -> x1, starting transfers between devices: none -> 4.96 us  [gather_turned(): lax.all_to_all(jnp.stack([both for _ in range(lax.axis_size(axis))], axis...]
where the time goes in v1:
time: 188 us
  waiting for transfers between devices  113 us (60%)
  blocking collectives  28.4 us (15%)
  between operations  14.3 us (8%)
  local copies, waits for them, and re-layouts  9.89 us (5%)
  starting transfers between devices  9.63 us (5%)
  matrix products  8.94 us (5%)
  other arithmetic  2.99 us (2%)
    all_to_all x1, waiting for transfers between devices, gather_turned(): lax.all_to_all(jnp.stack([both for _ in range(lax.axis_size(axis))], axis...  50.3 us
    all_gather x1, waiting for transfers between devices, side_by_side(): lax.all_gather(both, axis, axis=dim, tiled=True)  44.3 us
    all_to_all x1, blocking collectives, sum_at_owner(): tiles = lax.all_to_all(cut_along(x, dim, size), axis, 0, 0, tiled=True)  28.4 us
    all_to_all x1, waiting for transfers between devices, copy_for_each(): lax.all_to_all(jnp.broadcast_to(x[None], (size, *x.shape)), axis, 0, 0, t...  18.6 us
    all_to_all x1, starting transfers between devices, gather_turned(): lax.all_to_all(jnp.stack([both for _ in range(lax.axis_size(axis))], axis...  4.96 us
    dot_general x2, matrix products, contract_rows(): lax.dot_general(left, right, (((0,), (0,)), ((), ())), preferred_element_...  4.85 us
    all_to_all x1, starting transfers between devices, copy_for_each(): lax.all_to_all(jnp.broadcast_to(x[None], (size, *x.shape)), axis, 0, 0, t...  4.63 us
  transfers between devices with their start and end apart: 3, of which 3 were waited for; matrix products, arithmetic and copies ran while one was open for 2% of the time, Pallas kernels for 0%

profile of v1, /device:TPU:2, one launch (start us, length us, event | category | flops | bytes accessed | tf_op | source)
XLA Modules:
  0.0 187.5 jit_solution(9494529313948475233)
XLA Ops:
  7.2 0.0 copy-start
  7.2 0.0 copy-start.3
  7.2 0.0 copy-start.11
  7.2 0.0 copy-start.12
  7.2 0.0 all-gather.2.cloned.1.call-start
  7.3 1.9 %pad_maximum_fusion = bf16[1024,256]{1,0:T(8,128)(2,1)} fusion(bf16[512,256]{1,0:T(8,128)(2,1)} %param.21, bf16[512,256]{1,0:T(8,128)(2,1)} %param.15), kind=kLoop, calls=%fused_computation.16 | loop fusion | flops 1048576 | bytes 1048576 | tf_op jit(solution)/shard_map/concatenate | solution.py:13
  9.2 0.0 all-gather.2.cloned.1.call-update
  9.2 0.0 copy-start.2
  9.2 1.3 reshape.89
  10.5 0.0 copy-done.3
  10.5 0.3 reshape.90
  10.8 0.0 copy-done.11
  10.8 0.7 multiply_reduce_fusion
  11.5 0.0 copy-done.12
  11.5 0.1 broadcast_bitcast_fusion
  11.6 44.3 %all-gather.2.cloned.1.call-done = bf16[1024,2048]{1,0:T(8,128)(2,1)} async-done(((bf16[1024,256]{1,0:T(8,128)(2,1)}), bf16[1024,2048]{1,0:T(8,128)(2,1)}) %all-gather.2.cloned.1.call-update) | async-done | bytes 4194320 | tf_op jit(solution)/shard_map/all_gather | solution.py:14
  55.9 0.6 mul.124
  56.5 0.0 copy-done.2
  56.6 0.0 copy-start.1
  56.6 2.5 %convolution_multiply_fusion = f32[2048,256]{1,0:T(8,128)S(1)} fusion(bf16[1024,2048]{1,0:T(8,128)(2,1)} %all-gather.2.cloned.1.call-done, f32[64,8,2,128]{3,2,1,0:T(2,128)S(1)} %bitcast.27, f32[256]{0:T(256)S(1)} %get-tuple-element.51, f32[256]{0:T(256)S(1)} %get-tuple-element.52, bf16[512,256]{1,0:T(8,128)(2,1)S(1)} %copy-done.3, ...), kind=kOutput, calls=%fused_computation | convolution fusion | flops 538312704 | bytes 5244928 | tf_op jit(solution)/shard_map/dot_general | solution.py:72
  59.1 0.0 copy-done.1
  59.1 0.0 copy-start.13
  59.1 1.5 fusion.3
  60.7 0.0 copy-done.13
  60.7 2.3 %convolution_multiply_fusion.1 = f32[2048,256]{1,0:T(8,128)S(1)} fusion(bf16[512,256]{1,0:T(8,128)(2,1)S(1)} %copy-done.13, bf16[1024,2048]{1,0:T(8,128)(2,1)} %all-gather.2.cloned.1.call-done), kind=kOutput, calls=%fused_computation.1 | convolution fusion | flops 537395200 | bytes 4456448 | tf_op jit(solution)/shard_map/dot_general | solution.py:72
  63.0 0.0 copy-done
  63.0 0.0 copy-start.7
  63.0 0.0 copy-start.8
  63.1 0.0 copy-start.9
  63.1 0.0 copy-start.10
  63.1 1.5 fusion.2
  64.6 0.0 copy-start.5
  64.6 0.0 copy-start.6
  64.6 0.1 pad_maximum_fusion.1
  64.8 28.4 %all_to_all.15 = bf16[64,4,512]{2,1,0:T(4,128)(2,1)S(1)} all-to-all(bf16[64,4,512]{2,1,0:T(4,128)(2,1)S(1)} %pad_maximum_fusion.1), channel_id=1, replica_groups=mesh['fs'=64,'tp'=8] {'fs'}, dimensions={0} | all-to-all | bytes 524288 | tf_op jit(solution)/shard_map/all_to_all | solution.py:24
  93.2 0.1 convert_reduce_fusion
  93.3 0.0 copy-done.7
  93.3 0.0 copy-done.8
  93.3 0.0 copy-done.9
  93.3 0.0 copy-done.10
  93.4 0.9 broadcast_in_dim.2
  94.3 4.6 %all-to-all-start.1 = ((f32[64,4,512]{2,1,0:T(4,128)}), f32[64,4,512]{2,1,0:T(4,128)S(1)}, u32[]{:S(2)}, u32[]{:S(2)}) async-start(f32[64,4,512]{2,1,0:T(4,128)} %broadcast_in_dim.2), calls=%async_computation.1 | async-start | bytes 1048576 | tf_op jit(solution)/shard_map/all_to_all | solution.py:36
  98.9 18.6 %all-to-all-done.1 = f32[64,4,512]{2,1,0:T(4,128)S(1)} async-done(((f32[64,4,512]{2,1,0:T(4,128)}), f32[64,4,512]{2,1,0:T(4,128)S(1)}, u32[]{:S(2)}, u32[]{:S(2)}) %all-to-all-start.1) | async-done | bytes 524320 | tf_op jit(solution)/shard_map/all_to_all | solution.py:36
  117.5 0.2 reshape.91
  117.7 0.0 copy-done.5
  117.7 0.2 fusion.4
  118.0 0.0 copy-start.4
  118.0 0.0 copy-done.6
  118.0 0.9 fusion.25
  118.9 1.6 stack.2
  120.5 0.0 copy-done.4
  120.5 5.0 %all-to-all-start.2 = ((bf16[64,32,512]{2,1,0:T(8,128)(2,1)}), bf16[64,32,512]{2,1,0:T(8,128)(2,1)S(1)}, u32[]{:S(2)}, u32[]{:S(2)}) async-start(bf16[64,32,512]{2,1,0:T(8,128)(2,1)} %stack.2), calls=%async_computation.2 | async-start | bytes 4194304 | tf_op jit(solution)/shard_map/all_to_all | solution.py:48
  125.4 0.6 fusion.23
  126.0 0.6 fusion.24
  126.6 50.3 %all-to-all-done.2 = bf16[64,32,512]{2,1,0:T(8,128)(2,1)S(1)} async-done(((bf16[64,32,512]{2,1,0:T(8,128)(2,1)}), bf16[64,32,512]{2,1,0:T(8,128)(2,1)S(1)}, u32[]{:S(2)}, u32[]{:S(2)}) %all-to-all-start.2) | async-done | bytes 2097184 | tf_op jit(solution)/shard_map/all_to_all | solution.py:48
  177.0 1.5 slice_bitcast_fusion
  178.4 2.3 %copy.30 = bf16[256,2048]{1,0:T(8,128)(2,1)} copy(bf16[256,2048]{0,1:T(8,128)(2,1)} %get-tuple-element.43) | data formatting | bytes 2097152
  (6 shorter events, 0.2 us)
Async XLA Ops:
  7.2 55.9 %copy-start = (bf16[2048,256]{1,0:T(8,128)(2,1)S(1)}, bf16[2048,256]{1,0:T(8,128)(2,1)}, u32[]{:S(2)}) copy-start(bf16[2048,256]{1,0:T(8,128)(2,1)} %param.22) | copy-start | bytes 3145732
  7.2 3.3 %copy-start.3 = (bf16[512,256]{1,0:T(8,128)(2,1)S(1)}, bf16[512,256]{1,0:T(8,128)(2,1)}, u32[]{:S(2)}) copy-start(bf16[512,256]{1,0:T(8,128)(2,1)} %param.18) | copy-start | bytes 786436
  7.2 3.6 %copy-start.11 = (f32[2]{0:T(128)S(1)}, f32[2]{0:T(128)}, u32[]{:S(2)}) copy-start(f32[2]{0:T(128)} %param.19) | copy-start | bytes 28
  7.2 4.3 %copy-start.12 = (f32[128]{0:T(128)S(1)}, f32[128]{0:T(128)}, u32[]{:S(2)}) copy-start(f32[128]{0:T(128)} %param.20) | copy-start | bytes 1540
  7.2 48.7 %all-gather.2.cloned.1.call-start = ((), (), s32[]{:S(2)}) async-start(), calls=%async_computation.3 | async-start | bytes 4718592 | tf_op jit(solution)/shard_map/all_gather | solution.py:14
  9.2 47.3 %copy-start.2 = (bf16[512,256]{1,0:T(8,128)(2,1)S(1)}, bf16[512,256]{1,0:T(8,128)(2,1)}, u32[]{:S(2)}) copy-start(bf16[512,256]{1,0:T(8,128)(2,1)} %param.17) | copy-start | bytes 786436
  56.6 2.5 %copy-start.1 = (bf16[2048,256]{1,0:T(8,128)(2,1)S(1)}, bf16[2048,256]{1,0:T(8,128)(2,1)}, u32[]{:S(2)}) copy-start(bf16[2048,256]{1,0:T(8,128)(2,1)} %param.23) | copy-start | bytes 3145732
  59.1 1.6 copy-start.13
  63.0 30.3 %copy-start.7 = (f32[4,256]{1,0:T(4,128)S(1)}, f32[4,256]{1,0:T(4,128)}, u32[]{:S(2)}) copy-start(f32[4,256]{1,0:T(4,128)} %param.29) | copy-start | bytes 12292
  63.0 30.3 %copy-start.8 = (f32[4,256]{1,0:T(4,128)S(1)}, f32[4,256]{1,0:T(4,128)}, u32[]{:S(2)}) copy-start(f32[4,256]{1,0:T(4,128)} %param.27) | copy-start | bytes 12292
  63.1 30.3 %copy-start.9 = (f32[4,256]{1,0:T(4,128)S(1)}, f32[4,256]{1,0:T(4,128)}, u32[]{:S(2)}) copy-start(f32[4,256]{1,0:T(4,128)} %param.28) | copy-start | bytes 12292
  63.1 30.3 %copy-start.10 = (f32[4,256]{1,0:T(4,128)S(1)}, f32[4,256]{1,0:T(4,128)}, u32[]{:S(2)}) copy-start(f32[4,256]{1,0:T(4,128)} %param.26) | copy-start | bytes 12292
  64.6 53.2 %copy-start.5 = (f32[256,32]{0,1:T(8,128)S(1)}, f32[256,32]{0,1:T(8,128)}, u32[]{:S(2)}) copy-start(f32[256,32]{0,1:T(8,128)} %param.25) | copy-start | bytes 98308
  64.6 53.4 %copy-start.6 = (f32[32,256]{1,0:T(8,128)S(1)}, f32[32,256]{1,0:T(8,128)}, u32[]{:S(2)}) copy-start(f32[32,256]{1,0:T(8,128)} %param.24) | copy-start | bytes 98308
  94.3 23.3 %all-to-all-start.1 = ((f32[64,4,512]{2,1,0:T(4,128)}), f32[64,4,512]{2,1,0:T(4,128)S(1)}, u32[]{:S(2)}, u32[]{:S(2)}) async-start(f32[64,4,512]{2,1,0:T(4,128)} %broadcast_in_dim.2), calls=%async_computation.1 | async-start | bytes 1048576 | tf_op jit(solution)/shard_map/all_to_all | solution.py:36
  118.0 2.5 %copy-start.4 = (f32[256,32]{0,1:T(8,128)}, f32[256,32]{0,1:T(8,128)S(1)}, u32[]{:S(2)}) copy-start(f32[256,32]{0,1:T(8,128)S(1)} %fusion.4) | copy-start | bytes 98308
  120.5 56.5 %all-to-all-start.2 = ((bf16[64,32,512]{2,1,0:T(8,128)(2,1)}), bf16[64,32,512]{2,1,0:T(8,128)(2,1)S(1)}, u32[]{:S(2)}, u32[]{:S(2)}) async-start(bf16[64,32,512]{2,1,0:T(8,128)(2,1)} %stack.2), calls=%async_computation.2 | async-start | bytes 4194304 | tf_op jit(solution)/shard_map/all_to_all | solution.py:48
Sparse Core Ops, SparseCore 0:
  10.7 45.1 all-gather.1
